TPU v7x, 32 devices: a whole 2x2x4 slice. The times are simulated.
32 devices in a mesh: dp: 4 (over y, x), kv: 4 (over z), tp: 2 (over core).
Axes of the slice: x: 2, y: 2, z: 4, core: 2. Of those that a mesh axis runs over, the one named last changes fastest.
Arguments:
- tokens: bfloat16 [128, 2048], P('dp', ('kv', 'tp')), may hold values from -100 to 100
- delta_state: float32 [128, 8, 128, 128], P(('dp', 'kv'), 'tp'), may hold values from -0.6 to 0.6
- gain_in: bfloat16 [2048], P('kv'), may hold values from 0.099609375 to 1.8984375
- w_query: bfloat16 [2048, 1024], P('kv', 'tp'), may hold values from -0.125 to 0.125
- w_key: bfloat16 [2048, 1024], P('kv', 'tp'), may hold values from -0.125 to 0.125
- w_value: bfloat16 [2048, 1024], P('kv', 'tp'), may hold values from -0.125 to 0.125
- w_out_gate: bfloat16 [2048, 1024], P('kv', 'tp'), may hold values from -0.125 to 0.125
- w_beta: bfloat16 [2048, 8], P('kv'), may hold values from -0.125 to 0.125
- w_decay: bfloat16 [2048, 8], P('kv'), may hold values from -0.125 to 0.125
- decay_rate: float32 [8], P('tp'), may hold values from 0.05 to 3
- head_gain: float32 [128], replicated, may hold values from 0.1 to 1.9
- w_mix: bfloat16 [1024, 2048], P('tp', 'kv'), may hold values from -0.1875 to 0.1875
- gain_mid: bfloat16 [2048], P('kv'), may hold values from 0.099609375 to 1.8984375
- w_gate: bfloat16 [2048, 5632], P('tp', 'kv'), may hold values from -0.125 to 0.125
- w_up: bfloat16 [2048, 5632], P('tp', 'kv'), may hold values from -0.125 to 0.125
- w_down: bfloat16 [5632, 2048], P('kv', 'tp'), may hold values from -0.078125 to 0.078125
Outputs:
- layer_out: bfloat16 [128, 2048], P('dp', ('kv', 'tp'))
- next_state: float32 [128, 8, 128, 128], P(('dp', 'kv'), 'tp')
All inputs are finite; a program needn't handle non-finite values.
Results may differ from a plain program's by a relative error of at most 0.0095.
Values may be sent and summed in bfloat16 or wider, within the bound.
A program may use at most 64 MiB of HBM per device.

v0:
```python
import jax
import jax.numpy as jnp
from jax import lax
from jax.sharding import PartitionSpec as P

D = 2048
HEAD_DIM = 128
norm_epsilon = 1e-06


def unit_rows(vector):
    return vector * lax.rsqrt(jnp.sum(vector * vector, axis=-1, keepdims=True) + norm_epsilon)


def mixer_core(
    query_lin, key_lin, value_lin, gate_lin, beta_lin, decay_lin, delta_state, decay_rate, head_gain
):
    seq_count = query_lin.shape[0]
    head_count = beta_lin.shape[1]
    shaped = lambda matrix: matrix.reshape(seq_count, head_count, HEAD_DIM)
    query = unit_rows(jax.nn.silu(shaped(query_lin))) * HEAD_DIM ** (-0.5)
    key_vec = unit_rows(jax.nn.silu(shaped(key_lin)))
    value_vec = jax.nn.silu(shaped(value_lin))
    write_rate = jax.nn.sigmoid(beta_lin)
    keep_rate = jnp.exp(-decay_rate[None, :] * jax.nn.softplus(decay_lin))
    recalled = jnp.einsum("bhkv,bhk->bhv", delta_state, key_vec, precision=lax.Precision.HIGHEST)
    correction = write_rate[..., None] * (value_vec - keep_rate[..., None] * recalled)
    next_state = (
        keep_rate[..., None, None] * delta_state + key_vec[..., :, None] * correction[..., None, :]
    )
    readout = jnp.einsum("bhkv,bhk->bhv", next_state, query, precision=lax.Precision.HIGHEST)
    readout = readout * lax.rsqrt(
        jnp.mean(readout * readout, axis=-1, keepdims=True) + norm_epsilon
    )
    readout = readout * head_gain * jax.nn.silu(shaped(gate_lin))
    return (readout.reshape(seq_count, head_count * HEAD_DIM).astype(jnp.bfloat16), next_state)


def local(
    tokens,
    delta_state,
    gain_in,
    w_query,
    w_key,
    w_value,
    w_out_gate,
    w_beta,
    w_decay,
    decay_rate,
    head_gain,
    w_mix,
    gain_mid,
    w_gate,
    w_up,
    w_down,
):
    group_size = lax.axis_size("kv")
    group_pos = lax.axis_index("kv")
    core_pos = lax.axis_index("tp")
    all_rows = tokens.shape[0]
    own_rows = all_rows // group_size
    own_first = group_pos * own_rows
    feature_count = tokens.shape[1]
    head_count = w_query.shape[1] // HEAD_DIM
    width_dev = w_query.shape[1]
    token_float = tokens.astype(jnp.float32)
    sum_squares = jnp.sum(token_float * token_float, axis=1, keepdims=True)
    whole_rows, square_pair = (
        lax.all_gather(tokens, "tp", axis=1, tiled=True),
        lax.all_gather(sum_squares.astype(jnp.bfloat16), "tp", axis=1, tiled=True).astype(
            sum_squares.dtype
        ),
    )
    square_total = lax.psum(jnp.sum(square_pair, axis=1), "kv")
    row_scale = lax.rsqrt(square_total / D + norm_epsilon)
    normed = (whole_rows.astype(jnp.float32) * gain_in.astype(jnp.float32)).astype(jnp.bfloat16)
    beta_cols = lax.dynamic_slice_in_dim(w_beta, core_pos * head_count, head_count, 1)
    decay_cols = lax.dynamic_slice_in_dim(w_decay, core_pos * head_count, head_count, 1)
    row_block = normed
    results = [
        jnp.dot(row_block, weight, preferred_element_type=jnp.float32)
        for weight in (w_query, w_key, w_value, w_out_gate, beta_cols, decay_cols)
    ]
    summand = jnp.concatenate(results, axis=1)
    projected = lax.psum_scatter(
        summand.astype(jnp.bfloat16), "kv", scatter_dimension=0, tiled=True
    ).astype(jnp.float32)
    projected = projected * lax.dynamic_slice_in_dim(row_scale, own_first, own_rows, 0)[:, None]
    mixed, next_state = mixer_core(
        projected[:, :width_dev],
        projected[:, width_dev : 2 * width_dev],
        projected[:, 2 * width_dev : 3 * width_dev],
        projected[:, 3 * width_dev : 4 * width_dev],
        projected[:, 4 * width_dev : 4 * width_dev + head_count],
        projected[:, 4 * width_dev + head_count :],
        delta_state,
        decay_rate,
        head_gain,
    )
    attn_part = jnp.dot(
        lax.all_gather(mixed, "kv", axis=0, tiled=True), w_mix, preferred_element_type=jnp.float32
    )
    attn = lax.psum_scatter(
        attn_part.astype(jnp.bfloat16), "tp", scatter_dimension=1, tiled=True
    ).astype(jnp.float32)
    middle_own = (token_float + attn).astype(jnp.bfloat16)
    middle_float = middle_own.astype(jnp.float32)
    mid_squares = jnp.sum(middle_float * middle_float, axis=1, keepdims=True)
    gain_own = lax.dynamic_slice_in_dim(gain_mid, core_pos * feature_count, feature_count, 0)
    normed_own = (middle_float * gain_own.astype(jnp.float32)).astype(jnp.bfloat16)
    normed_half, square_parts = (
        lax.all_gather(normed_own, "kv", axis=1, tiled=True),
        lax.all_gather(mid_squares.astype(jnp.bfloat16), "kv", axis=1, tiled=True).astype(
            mid_squares.dtype
        ),
    )
    mid_total = lax.psum(jnp.sum(square_parts, axis=1), "tp")
    mid_scale = lax.rsqrt(mid_total / D + norm_epsilon)
    hidden_dev = w_gate.shape[1]
    row_block = normed_half
    summand = jnp.concatenate(
        [
            jnp.dot(row_block, w_gate, preferred_element_type=jnp.float32),
            jnp.dot(row_block, w_up, preferred_element_type=jnp.float32),
        ],
        axis=1,
    )
    gate_up = lax.psum(summand.astype(jnp.bfloat16), "tp").astype(jnp.float32)
    gate_up = gate_up * mid_scale[:, None]
    activated = (jax.nn.silu(gate_up[:, :hidden_dev]) * gate_up[:, hidden_dev:]).astype(
        jnp.bfloat16
    )
    down_local = jnp.dot(activated, w_down, preferred_element_type=jnp.float32)
    down_part = lax.psum_scatter(
        down_local.astype(jnp.bfloat16), "kv", scatter_dimension=1, tiled=True
    ).astype(jnp.float32)
    layer_out = (middle_float + down_part).astype(jnp.bfloat16)
    return (layer_out, next_state)


def solution(mesh):
    in_specs = (
        P("dp", ("kv", "tp")),
        P(("dp", "kv"), "tp", None, None),
        P("kv"),
        P("kv", "tp"),
        P("kv", "tp"),
        P("kv", "tp"),
        P("kv", "tp"),
        P("kv", None),
        P("kv", None),
        P("tp"),
        P(),
        P("tp", "kv"),
        P("kv"),
        P("tp", "kv"),
        P("tp", "kv"),
        P("kv", "tp"),
    )
    out_specs = (P("dp", ("kv", "tp")), P(("dp", "kv"), "tp", None, None))
    return jax.shard_map(local, mesh=mesh, in_specs=in_specs, out_specs=out_specs, check_vma=False)
```

profile of v0, /device:TPU:0, one launch (start us, length us, event | category | flops | bytes accessed | tf_op | source)
XLA Modules:
  0.0 164.7 jit_solution(10898741676465725415)
XLA Ops:
  7.3 0.8 convert_element_type.92
  8.1 2.3 %all_gather.15 = bf16[32,512]{1,0:T(8,128)(2,1)S(1)} all-gather(bf16[32,256]{1,0:T(8,128)(2,1)} %param.16), channel_id=1, replica_groups=mesh['dp'=4,'kv'=4,'tp'=2] {'tp'}, dimensions={1}, use_global_device_ids=true | all-gather | bytes 49152 | tf_op jit(solution)/shard_map/all_gather | solution.py:69
  10.4 0.8 convolution_convert_fusion.9
  11.2 0.8 convolution_convert_fusion.8
  12.3 1.2 convolution_convert_fusion.6
  13.5 1.2 convolution_convert_fusion.5
  14.7 1.2 convolution_convert_fusion.4
  16.0 1.2 convolution_convert_fusion.7
  17.2 0.8 concatenate.8
  18.2 1.8 %all-gather = bf16[2,1,32]{2,1,0:T(2,128)(2,1)S(1)} all-gather(bf16[1,1,32]{2,1,0:T(2,128)(2,1)S(1)} %bitcast.72), channel_id=1, replica_groups=mesh['dp'=4,'kv'=4,'tp'=2] {'tp'}, dimensions={0}, use_global_device_ids=true | all-gather | bytes 192 | tf_op jit(solution)/shard_map/all_gather | solution.py:70
  20.0 13.3 %psum.21 = f32[32]{0:T(128)S(1)} all-reduce(f32[32]{0:T(128)S(1)} %convert_reduce_fusion.1), channel_id=1, replica_groups=mesh['dp'=4,'kv'=4,'tp'=2] {'kv'}, use_global_device_ids=true, to_apply=%region_3.0 | all-reduce | flops 32 | bytes 256 | tf_op jit(solution)/shard_map/psum | solution.py:74
  34.7 20.7 %all-reduce.6.cloned.1.call-done = bf16[32,2056]{1,0:T(8,128)(2,1)} async-done(((bf16[32,2056]{1,0:T(8,128)(2,1)}), bf16[32,2056]{1,0:T(8,128)(2,1)}) %all-reduce.6.cloned.1.call-update) | async-done | bytes 131600
  55.4 0.8 convert_multiply_fusion.1
  56.7 3.6 %fusion.16 = f32[8,4,1,128]{3,2,1,0:T(1,128)S(1)} fusion(f32[8,4,128,128]{3,2,1,0:T(8,128)} %param.17, f32[8,4,128,1]{2,0,1,3:T(8,128)S(1)} %bitcast.70), kind=kOutput, calls=%fused_computation.43 | convolution fusion | flops 6291456 | bytes 2129920 | tf_op jit(solution)/shard_map/bhkv,bhk->bhv/dot_general | solution.py:26
  60.3 0.8 multiply_add_fusion
  61.1 1.3 copy-done.2
  62.4 1.9 %fusion.14 = f32[8,4,1,128]{3,2,1,0:T(1,128)S(1)} fusion(f32[8,4,128,128]{3,2,1,0:T(8,128)S(1)} %multiply_add_fusion, f32[8,4,128,1]{2,0,1,3:T(8,128)S(1)} %get-tuple-element.4), kind=kOutput, calls=%fused_computation.41 | convolution fusion | flops 6291456 | bytes 2129920 | tf_op jit(solution)/shard_map/bhkv,bhk->bhv/dot_general | solution.py:31
  64.5 13.1 %all_gather.17 = bf16[32,512]{1,0:T(8,128)(2,1)S(1)} all-gather(bf16[8,512]{1,0:T(8,128)(2,1)S(1)} %fusion.18), channel_id=1, replica_groups=mesh['dp'=4,'kv'=4,'tp'=2] {'kv'}, dimensions={0}, use_global_device_ids=true | all-gather | bytes 40960 | tf_op jit(solution)/shard_map/all_gather | solution.py:101
  77.6 0.8 convolution_convert_fusion.3
  78.6 7.6 %reduce-scatter.3.cloned.1.call-done = bf16[32,256]{1,0:T(8,128)(2,1)} async-done(((bf16[32,512]{1,0:T(8,128)(2,1)}), bf16[32,256]{1,0:T(8,128)(2,1)}) %reduce-scatter.3.cloned.1.call-update) | async-done | bytes 16400 | tf_op jit(solution)/shard_map/reduce_scatter | solution.py:103
  86.2 0.8 fusion.6
  87.0 11.1 %all-gather.1 = bf16[4,1,32]{2,1,0:T(2,128)(2,1)S(1)} all-gather(bf16[1,1,32]{2,1,0:T(2,128)(2,1)S(1)} %bitcast.71), channel_id=1, replica_groups=mesh['dp'=4,'kv'=4,'tp'=2] {'kv'}, dimensions={0}, use_global_device_ids=true | all-gather | bytes 320 | tf_op jit(solution)/shard_map/all_gather | solution.py:113
  98.1 2.5 %psum.23 = f32[32]{0:T(128)S(1)} all-reduce(f32[32]{0:T(128)S(1)} %convert_reduce_fusion), channel_id=1, replica_groups=mesh['dp'=4,'kv'=4,'tp'=2] {'tp'}, use_global_device_ids=true, to_apply=%region_11.12 | all-reduce | flops 32 | bytes 256 | tf_op jit(solution)/shard_map/psum | solution.py:117
  100.6 13.2 %all_gather.18 = bf16[32,1024]{1,0:T(8,128)(2,1)S(1)} all-gather(bf16[32,256]{1,0:T(8,128)(2,1)S(1)} %get-tuple-element.9), channel_id=1, replica_groups=mesh['dp'=4,'kv'=4,'tp'=2] {'kv'}, dimensions={1}, use_global_device_ids=true | all-gather | bytes 81920 | tf_op jit(solution)/shard_map/all_gather | solution.py:112
  113.8 0.6 convolution_convert_fusion
  114.4 0.6 convolution_convert_fusion.1
  115.0 0.7 pad_maximum_fusion
  115.8 16.3 %all-reduce.4.cloned.1.call-done = bf16[32,2816]{1,0:T(8,128)(2,1)} async-done(((bf16[32,2816]{1,0:T(8,128)(2,1)}), bf16[32,2816]{1,0:T(8,128)(2,1)}) %all-reduce.4.cloned.1.call-update) | async-done | bytes 180240 | tf_op jit(solution)/shard_map/psum | solution.py:128
  132.1 1.0 convert_multiply_fusion
  133.1 3.0 %convolution_convert_fusion.2 = bf16[32,1024]{1,0:T(8,128)(2,1)} fusion(bf16[1408,1024]{1,0:T(8,128)(2,1)} %param.31, f32[32,2816]{1,0:T(8,128)S(1)} %convert_multiply_fusion), kind=kOutput, calls=%fused_computation.3 | convolution fusion | flops 92577792 | bytes 3309568 | tf_op jit(solution)/shard_map/dot_general | solution.py:133
  136.2 20.7 %reduce-scatter.5.cloned.1.call-done = bf16[32,256]{1,0:T(8,128)(2,1)} async-done(((bf16[32,1024]{1,0:T(8,128)(2,1)}), bf16[32,256]{1,0:T(8,128)(2,1)}) %reduce-scatter.5.cloned.1.call-update) | async-done | bytes 16400 | tf_op jit(solution)/shard_map/reduce_scatter | solution.py:134
  156.8 1.3 fusion.7
  (52 shorter events, 2.1 us)
Async XLA Ops:
  7.2 106.7 %copy-start = (bf16[1024,1408]{1,0:T(8,128)(2,1)S(1)}, bf16[1024,1408]{1,0:T(8,128)(2,1)}, u32[]{:S(2)}) copy-start(bf16[1024,1408]{1,0:T(8,128)(2,1)} %param.30) | copy-start | bytes 8650756
  7.2 26.2 %copy-start.10 = (u32[32]{0:T(128)S(1)}, u32[32]{0:T(128)}, u32[]{:S(2)}) copy-start(u32[32]{0:T(128)} %constant.48) | copy-start | bytes 388
  7.2 10.9 %copy-start.5 = (bf16[32,256]{1,0:T(8,128)(2,1)S(1)}, bf16[32,256]{1,0:T(8,128)(2,1)}, u32[]{:S(2)}) copy-start(bf16[32,256]{1,0:T(8,128)(2,1)} %param.16) | copy-start | bytes 49156
  7.2 11.0 %copy-start.9 = (f32[4]{0:T(128)S(1)}, f32[4]{0:T(128)}, u32[]{:S(2)}) copy-start(f32[4]{0:T(128)} %param.25) | copy-start | bytes 52
  7.2 48.2 %all-reduce.6.cloned.1.call-start = ((), (), s32[]{:S(2)}) async-start(), calls=%async_computation.5 | async-start | bytes 278528
  18.0 68.2 %reduce-scatter.3.cloned.1.call-start = ((), (), s32[]{:S(2)}) async-start(), calls=%async_computation.2 | async-start | bytes 49152 | tf_op jit(solution)/shard_map/reduce_scatter | solution.py:103
  56.6 3.8 %copy-start.1 = (f32[8,4,128,128]{3,2,1,0:T(8,128)S(1)}, f32[8,4,128,128]{3,2,1,0:T(8,128)}, u32[]{:S(2)}) copy-start(f32[8,4,128,128]{3,2,1,0:T(8,128)} %param.17) | copy-start | bytes 6291460
  61.1 1.3 copy-start.2
  61.1 3.3 %copy-start.7 = (f32[128]{0:T(128)S(1)}, f32[128]{0:T(128)}, u32[]{:S(2)}) copy-start(f32[128]{0:T(128)} %param.26) | copy-start | bytes 1540
  61.1 16.5 %copy-start.4 = (bf16[512,512]{1,0:T(8,128)(2,1)S(1)}, bf16[512,512]{1,0:T(8,128)(2,1)}, u32[]{:S(2)}) copy-start(bf16[512,512]{1,0:T(8,128)(2,1)} %param.27) | copy-start | bytes 1572868
  61.1 17.4 %copy-start.8 = (bf16[512]{0:T(512)(128)(2,1)S(1)}, bf16[512]{0:T(512)(128)(2,1)}, u32[]{:S(2)}) copy-start(bf16[512]{0:T(512)(128)(2,1)} %param.28) | copy-start | bytes 3076
  78.5 53.7 %all-reduce.4.cloned.1.call-start = ((), (), s32[]{:S(2)}) async-start(), calls=%async_computation.3 | async-start | bytes 360448 | tf_op jit(solution)/shard_map/psum | solution.py:128
  100.6 13.8 %copy-start.3 = (bf16[1024,1408]{1,0:T(8,128)(2,1)S(1)}, bf16[1024,1408]{1,0:T(8,128)(2,1)}, u32[]{:S(2)}) copy-start(bf16[1024,1408]{1,0:T(8,128)(2,1)} %param.29) | copy-start | bytes 8650756
  115.0 41.8 %copy-start.6 = (bf16[32,256]{1,0:T(8,128)(2,1)S(1)}, bf16[32,256]{1,0:T(8,128)(2,1)}, u32[]{:S(2)}) copy-start(bf16[32,256]{1,0:T(8,128)(2,1)} %reduce-scatter.3.cloned.1.call-done) | copy-start | bytes 49156
  115.7 41.1 %reduce-scatter.5.cloned.1.call-start = ((), (), s32[]{:S(2)}) async-start(), calls=%async_computation.4 | async-start | bytes 81920 | tf_op jit(solution)/shard_map/reduce_scatter | solution.py:134
Sparse Core Ops, SparseCore 0:
  18.1 37.2 all-reduce.5
  78.6 7.5 reduce-scatter.2
  115.9 16.1 all-reduce.3
  136.3 20.4 reduce-scatter.4
where the time goes:
time: 165 us
  waiting for transfers between devices  65.3 us (40%)
  blocking collectives  57.3 us (35%)
  matrix products  17 us (10%)
  between operations  14.6 us (9%)
  other arithmetic  7.06 us (4%)
  local copies, waits for them, and re-layouts  3.14 us (2%)
    unnamed x5, waiting for transfers between devices  20.8 us
    reduce_scatter x1, waiting for transfers between devices, local(): lax.psum_scatter(down_local.astype(jnp.bfloat16), 'kv', scatter_dimension...  20.7 us
    psum x1, waiting for transfers between devices, local(): gate_up = lax.psum(summand.astype(jnp.bfloat16), 'tp').astype(jnp.float32)  16.3 us
    psum x1, blocking collectives, local(): square_total = lax.psum(jnp.sum(square_pair, axis=1), 'kv')  13.3 us
    all_gather x1, blocking collectives, local(): lax.all_gather(normed_own, 'kv', axis=1, tiled=True)  13.2 us
    all_gather x1, blocking collectives, local(): lax.all_gather(mixed, 'kv', axis=0, tiled=True)  13.1 us
    all_gather x1, blocking collectives, local(): lax.all_gather(mid_squares.astype(jnp.bfloat16), 'kv', axis=1, tiled=True)  11.1 us
    reduce_scatter x1, waiting for transfers between devices, local(): lax.psum_scatter(attn_part.astype(jnp.bfloat16), 'tp', scatter_dimension=...  7.59 us
  transfers between devices with their start and end apart: 4, of which 4 were waited for; matrix products, arithmetic and copies ran while one was open for 1% of the time, Pallas kernels for 0%

commit v1 on v0

--- a/solution.py
+++ b/solution.py
@@ -125,7 +125,9 @@
         ],
         axis=1,
     )
-    gate_up = lax.psum(summand.astype(jnp.bfloat16), "tp").astype(jnp.float32)
+    gate_up = jnp.sum(lax.all_gather(summand.astype(jnp.bfloat16), "tp"), axis=0).astype(
+        jnp.float32
+    )
     gate_up = gate_up * mid_scale[:, None]
     activated = (jax.nn.silu(gate_up[:, :hidden_dev]) * gate_up[:, hidden_dev:]).astype(
         jnp.bfloat16

time: 165 us -> 147 us (0.89)
  waiting for transfers between devices: 65.3 us -> 46 us
  blocking collectives: 57.3 us -> 59.4 us
    psum x1 -> x0, waiting for transfers between devices: 16.3 us -> none  [local(): gate_up = lax.psum(summand.astype(jnp.bfloat16), 'tp').astype(jnp.float32)]
    reduce_scatter x1, waiting for transfers between devices: 20.7 us -> 17.6 us  [local(): lax.psum_scatter(down_local.astype(jnp.bfloat16), 'kv', scatter_dimension...]
    all_gather x0 -> x1, blocking collectives: none -> 2.06 us  [local(): lax.all_gather(summand.astype(jnp.bfloat16), 'tp')]
    unnamed x5 -> x4, waiting for transfers between devices: 20.8 us -> 20.8 us
  transfers between devices with their start and end apart: 4 -> 3, of which waited for: 4 -> 3; matrix products, arithmetic and copies ran while one was open for 1% -> 1% of each run, Pallas kernels for 0% -> 0%
where the time goes in v1:
time: 147 us; the launch traced here: 146 us
  blocking collectives  59.4 us (40%)
  waiting for transfers between devices  46 us (31%)
  matrix products  17 us (12%)
  between operations  14.6 us (10%)
  other arithmetic  5.56 us (4%)
  local copies, waits for them, and re-layouts  3.14 us (2%)
    unnamed x4, waiting for transfers between devices  20.8 us
    reduce_scatter x1, waiting for transfers between devices, local(): lax.psum_scatter(down_local.astype(jnp.bfloat16), 'kv', scatter_dimension...  17.6 us
    psum x1, blocking collectives, local(): square_total = lax.psum(jnp.sum(square_pair, axis=1), 'kv')  13.3 us
    all_gather x1, blocking collectives, local(): lax.all_gather(normed_own, 'kv', axis=1, tiled=True)  13.3 us
    all_gather x1, blocking collectives, local(): lax.all_gather(mixed, 'kv', axis=0, tiled=True)  13.1 us
    all_gather x1, blocking collectives, local(): lax.all_gather(mid_squares.astype(jnp.bfloat16), 'kv', axis=1, tiled=True)  11.1 us
    reduce_scatter x1, waiting for transfers between devices, local(): lax.psum_scatter(attn_part.astype(jnp.bfloat16), 'tp', scatter_dimension=...  7.59 us
    dot_general x6, matrix products, local(): jnp.dot(row_block, weight, preferred_element_type=jnp.float32)  6.6 us
  transfers between devices with their start and end apart: 3, of which 3 were waited for; matrix products, arithmetic and copies ran while one was open for 1% of the time, Pallas kernels for 0%

profile of v1, /device:TPU:0, one launch (start us, length us, event | category | flops | bytes accessed | tf_op | source)
XLA Modules:
  0.0 145.9 jit_solution(14273505552138581751)
XLA Ops:
  7.3 0.8 convert_element_type.101
  8.1 2.3 %all_gather.19 = bf16[32,512]{1,0:T(8,128)(2,1)S(1)} all-gather(bf16[32,256]{1,0:T(8,128)(2,1)} %param.16), channel_id=1, replica_groups=mesh['dp'=4,'kv'=4,'tp'=2] {'tp'}, dimensions={1}, use_global_device_ids=true | all-gather | bytes 49152 | tf_op jit(solution)/shard_map/all_gather | solution.py:69
  10.4 0.8 convolution_convert_fusion.9
  11.2 0.8 convolution_convert_fusion.8
  12.3 1.2 convolution_convert_fusion.6
  13.5 1.2 convolution_convert_fusion.5
  14.7 1.2 convolution_convert_fusion.4
  16.0 1.2 convolution_convert_fusion.7
  17.2 0.8 concatenate.19
  18.1 0.1 fusion.5
  18.2 1.8 %all-gather = bf16[2,1,32]{2,1,0:T(2,128)(2,1)S(1)} all-gather(bf16[1,1,32]{2,1,0:T(2,128)(2,1)S(1)} %bitcast.76), channel_id=1, replica_groups=mesh['dp'=4,'kv'=4,'tp'=2] {'tp'}, dimensions={0}, use_global_device_ids=true | all-gather | bytes 192 | tf_op jit(solution)/shard_map/all_gather | solution.py:70
  20.0 13.3 %psum.14 = f32[32]{0:T(128)S(1)} all-reduce(f32[32]{0:T(128)S(1)} %convert_reduce_fusion.1), channel_id=1, replica_groups=mesh['dp'=4,'kv'=4,'tp'=2] {'kv'}, use_global_device_ids=true, to_apply=%region_3.0 | all-reduce | flops 32 | bytes 256 | tf_op jit(solution)/shard_map/psum | solution.py:74
  33.3 0.6 dynamic-slice
  34.7 20.7 %all-reduce.3.cloned.1.call-done = bf16[32,2056]{1,0:T(8,128)(2,1)} async-done(((bf16[32,2056]{1,0:T(8,128)(2,1)}), bf16[32,2056]{1,0:T(8,128)(2,1)}) %all-reduce.3.cloned.1.call-update) | async-done | bytes 131600
  55.4 0.8 convert_multiply_fusion.1
  56.7 3.6 %fusion.18 = f32[8,4,1,128]{3,2,1,0:T(1,128)S(1)} fusion(f32[8,4,128,128]{3,2,1,0:T(8,128)} %param.17, f32[8,4,128,1]{2,0,1,3:T(8,128)S(1)} %bitcast.74), kind=kOutput, calls=%fused_computation.45 | convolution fusion | flops 6291456 | bytes 2129920 | tf_op jit(solution)/shard_map/bhkv,bhk->bhv/dot_general | solution.py:26
  60.3 0.8 multiply_add_fusion
  61.1 1.3 copy-done.2
  62.4 1.9 %fusion.16 = f32[8,4,1,128]{3,2,1,0:T(1,128)S(1)} fusion(f32[8,4,128,128]{3,2,1,0:T(8,128)S(1)} %multiply_add_fusion, f32[8,4,128,1]{2,0,1,3:T(8,128)S(1)} %get-tuple-element.4), kind=kOutput, calls=%fused_computation.43 | convolution fusion | flops 6291456 | bytes 2129920 | tf_op jit(solution)/shard_map/bhkv,bhk->bhv/dot_general | solution.py:31
  64.5 13.1 %all_gather.21 = bf16[32,512]{1,0:T(8,128)(2,1)S(1)} all-gather(bf16[8,512]{1,0:T(8,128)(2,1)S(1)} %fusion.20), channel_id=1, replica_groups=mesh['dp'=4,'kv'=4,'tp'=2] {'kv'}, dimensions={0}, use_global_device_ids=true | all-gather | bytes 40960 | tf_op jit(solution)/shard_map/all_gather | solution.py:101
  77.6 0.8 convolution_convert_fusion.3
  78.6 7.6 %reduce-scatter.3.cloned.1.call-done = bf16[32,256]{1,0:T(8,128)(2,1)} async-done(((bf16[32,512]{1,0:T(8,128)(2,1)}), bf16[32,256]{1,0:T(8,128)(2,1)}) %reduce-scatter.3.cloned.1.call-update) | async-done | bytes 16400 | tf_op jit(solution)/shard_map/reduce_scatter | solution.py:103
  86.2 0.8 fusion.8
  87.0 11.1 %all-gather.1 = bf16[4,1,32]{2,1,0:T(2,128)(2,1)S(1)} all-gather(bf16[1,1,32]{2,1,0:T(2,128)(2,1)S(1)} %bitcast.75), channel_id=1, replica_groups=mesh['dp'=4,'kv'=4,'tp'=2] {'kv'}, dimensions={0}, use_global_device_ids=true | all-gather | bytes 320 | tf_op jit(solution)/shard_map/all_gather | solution.py:113
  98.1 2.5 %psum.15 = f32[32]{0:T(128)S(1)} all-reduce(f32[32]{0:T(128)S(1)} %convert_reduce_fusion), channel_id=1, replica_groups=mesh['dp'=4,'kv'=4,'tp'=2] {'tp'}, use_global_device_ids=true, to_apply=%region_11.12 | all-reduce | flops 32 | bytes 256 | tf_op jit(solution)/shard_map/psum | solution.py:117
  100.6 13.3 %all_gather.22 = bf16[32,1024]{1,0:T(8,128)(2,1)S(1)} all-gather(bf16[32,256]{1,0:T(8,128)(2,1)S(1)} %get-tuple-element.9), channel_id=1, replica_groups=mesh['dp'=4,'kv'=4,'tp'=2] {'kv'}, dimensions={1}, use_global_device_ids=true | all-gather | bytes 81920 | tf_op jit(solution)/shard_map/all_gather | solution.py:112
  113.8 0.6 fusion.1
  114.4 0.6 fusion
  115.1 2.1 %all_gather.23 = bf16[2,32,2816]{2,1,0:T(8,128)(2,1)S(1)} all-gather(bf16[1,32,2816]{2,1,0:T(8,128)(2,1)S(1)} %pad_maximum_fusion), channel_id=1, replica_groups=mesh['dp'=4,'kv'=4,'tp'=2] {'tp'}, dimensions={0}, use_global_device_ids=true | all-gather | bytes 540672 | tf_op jit(solution)/shard_map/all_gather | solution.py:128
  117.3 3.0 %convolution_convert_fusion.2 = bf16[32,1024]{1,0:T(8,128)(2,1)} fusion(bf16[1408,1024]{1,0:T(8,128)(2,1)} %param.31, f32[32,2816]{1,0:T(8,128)S(1)} %convert_multiply_fusion), kind=kOutput, calls=%fused_computation.5 | convolution fusion | flops 92577792 | bytes 3309568 | tf_op jit(solution)/shard_map/dot_general | solution.py:135
  120.4 17.6 %reduce-scatter.5.cloned.1.call-done = bf16[32,256]{1,0:T(8,128)(2,1)} async-done(((bf16[32,1024]{1,0:T(8,128)(2,1)}), bf16[32,256]{1,0:T(8,128)(2,1)}) %reduce-scatter.5.cloned.1.call-update) | async-done | bytes 16400 | tf_op jit(solution)/shard_map/reduce_scatter | solution.py:136
  138.0 1.3 fusion.9
  (51 shorter events, 1.6 us)
Async XLA Ops:
  7.2 106.7 %copy-start = (bf16[1024,1408]{1,0:T(8,128)(2,1)S(1)}, bf16[1024,1408]{1,0:T(8,128)(2,1)}, u32[]{:S(2)}) copy-start(bf16[1024,1408]{1,0:T(8,128)(2,1)} %param.30) | copy-start | bytes 8650756
  7.2 26.2 %copy-start.10 = (u32[32]{0:T(128)S(1)}, u32[32]{0:T(128)}, u32[]{:S(2)}) copy-start(u32[32]{0:T(128)} %constant.50) | copy-start | bytes 388
  7.2 10.9 %copy-start.5 = (bf16[32,256]{1,0:T(8,128)(2,1)S(1)}, bf16[32,256]{1,0:T(8,128)(2,1)}, u32[]{:S(2)}) copy-start(bf16[32,256]{1,0:T(8,128)(2,1)} %param.16) | copy-start | bytes 49156
  7.2 11.0 %copy-start.9 = (f32[4]{0:T(128)S(1)}, f32[4]{0:T(128)}, u32[]{:S(2)}) copy-start(f32[4]{0:T(128)} %param.25) | copy-start | bytes 52
  7.2 48.2 %all-reduce.3.cloned.1.call-start = ((), (), s32[]{:S(2)}) async-start(), calls=%async_computation.4 | async-start | bytes 278528
  18.0 68.2 %reduce-scatter.3.cloned.1.call-start = ((), (), s32[]{:S(2)}) async-start(), calls=%async_computation.2 | async-start | bytes 49152 | tf_op jit(solution)/shard_map/reduce_scatter | solution.py:103
  56.6 3.8 %copy-start.1 = (f32[8,4,128,128]{3,2,1,0:T(8,128)S(1)}, f32[8,4,128,128]{3,2,1,0:T(8,128)}, u32[]{:S(2)}) copy-start(f32[8,4,128,128]{3,2,1,0:T(8,128)} %param.17) | copy-start | bytes 6291460
  61.1 1.3 copy-start.2
  61.1 3.3 %copy-start.7 = (f32[128]{0:T(128)S(1)}, f32[128]{0:T(128)}, u32[]{:S(2)}) copy-start(f32[128]{0:T(128)} %param.26) | copy-start | bytes 1540
  61.1 16.5 %copy-start.4 = (bf16[512,512]{1,0:T(8,128)(2,1)S(1)}, bf16[512,512]{1,0:T(8,128)(2,1)}, u32[]{:S(2)}) copy-start(bf16[512,512]{1,0:T(8,128)(2,1)} %param.27) | copy-start | bytes 1572868
  61.1 17.4 %copy-start.8 = (bf16[512]{0:T(512)(128)(2,1)S(1)}, bf16[512]{0:T(512)(128)(2,1)}, u32[]{:S(2)}) copy-start(bf16[512]{0:T(512)(128)(2,1)} %param.28) | copy-start | bytes 3076
  78.5 59.6 %reduce-scatter.5.cloned.1.call-start = ((), (), s32[]{:S(2)}) async-start(), calls=%async_computation.3 | async-start | bytes 81920 | tf_op jit(solution)/shard_map/reduce_scatter | solution.py:136
  100.6 13.9 %copy-start.3 = (bf16[1024,1408]{1,0:T(8,128)(2,1)S(1)}, bf16[1024,1408]{1,0:T(8,128)(2,1)}, u32[]{:S(2)}) copy-start(bf16[1024,1408]{1,0:T(8,128)(2,1)} %param.29) | copy-start | bytes 8650756
  117.1 20.9 %copy-start.6 = (bf16[32,256]{1,0:T(8,128)(2,1)S(1)}, bf16[32,256]{1,0:T(8,128)(2,1)}, u32[]{:S(2)}) copy-start(bf16[32,256]{1,0:T(8,128)(2,1)} %reduce-scatter.3.cloned.1.call-done) | copy-start | bytes 49156
Sparse Core Ops, SparseCore 0:
  18.1 37.2 all-reduce.2
  78.6 7.5 reduce-scatter.2
  120.5 17.4 reduce-scatter.4
